TPU v7x, 32 devices: a whole 2x2x4 slice. The times are simulated.
32 devices in a mesh: rep: 2 (over x), fs: 8 (over z, y), tp: 2 (over core).
Axes of the slice: x: 2, y: 2, z: 4, core: 2. Of those that a mesh axis runs over, the one named last changes fastest.
Arguments:
- tokens: bfloat16 [12288, 2048], P(('rep', 'fs')), may hold values from -6 to 6
- norm_gain: float32 [2048], replicated, may hold values from 0.1 to 1.9
- up_weight: bfloat16 [2048, 8192], P('fs', 'tp'), may hold values from -0.125 to 0.125
- down_weight: bfloat16 [8192, 2048], P('tp', 'fs'), may hold values from -0.0625 to 0.0625
Outputs:
- layer_out: bfloat16 [12288, 2048], P(('rep', 'fs'), 'tp')
All inputs are finite; a program needn't handle non-finite values.
Results may differ from a plain program's by a relative error of at most 0.013.
Values may be sent and summed in bfloat16 or wider, within the bound.
A program may use at most 128 MiB of HBM per device.

v0:
```python
import jax
import jax.numpy as jnp
from jax import lax
from jax.sharding import PartitionSpec as P


def local(tokens, norm_gain, up_weight, down_weight):
    xf = tokens.astype(jnp.float32)
    inv_rms = lax.rsqrt(jnp.mean(xf * xf, axis=-1, keepdims=True) + 1e-06)
    normed = (xf * inv_rms * norm_gain).astype(jnp.bfloat16)
    pre = jnp.dot(
        normed,
        lax.all_gather(up_weight, "fs", axis=0, tiled=True),
        preferred_element_type=jnp.float32,
    )
    hidden = jnp.square(jax.nn.relu(pre)).astype(jnp.bfloat16)
    terms = jnp.dot(
        hidden,
        lax.all_gather(down_weight, "fs", axis=1, tiled=True),
        preferred_element_type=jnp.float32,
    )
    summed = lax.psum_scatter(
        terms.astype(jnp.bfloat16), "tp", scatter_dimension=1, tiled=True
    ).astype(jnp.float32)
    width = summed.shape[1]
    own_cols = lax.dynamic_slice_in_dim(xf, lax.axis_index("tp") * width, width, 1)
    return (own_cols + summed).astype(jnp.bfloat16)


def solution(mesh):
    placed = (P(("rep", "fs"), None), P(), P("fs", "tp"), P("tp", "fs"))
    return jax.shard_map(
        local, mesh=mesh, in_specs=placed, out_specs=P(("rep", "fs"), "tp"), check_vma=False
    )
```

profile of v0, /device:TPU:0, one launch (start us, length us, event | category | flops | bytes accessed | tf_op | source)
XLA Modules:
  0.0 525.2 jit_solution(4391572638668240100)
XLA Ops:
  6.5 0.0 copy-start
  6.5 0.0 copy-start.1
  6.5 0.0 all-gather.5.cloned.1.call-start
  6.5 0.7 all-gather.5.cloned.1.call-update
  7.3 0.0 all-gather.3.cloned.1.call-start
  7.3 0.7 all-gather.3.cloned.1.call-update
  8.0 0.0 reduce-scatter.2.cloned.1.call-start
  8.1 0.4 copy-done
  8.4 0.7 multiply_reduce_fusion
  9.1 230.3 %all-gather.5.cloned.1.call-done = bf16[4096,2048]{1,0:T(8,128)(2,1)} async-done(((bf16[4096,256]{1,0:T(8,128)(2,1)}), bf16[4096,2048]{1,0:T(8,128)(2,1)}) %all-gather.5.cloned.1.call-update) | async-done | bytes 16777232 | tf_op jit(solution)/shard_map/all_gather | solution.py:19
  239.4 227.6 %all-gather.3.cloned.1.call-done = bf16[2048,4096]{1,0:T(8,128)(2,1)} async-done(((bf16[256,4096]{1,0:T(8,128)(2,1)}), bf16[2048,4096]{1,0:T(8,128)(2,1)}) %all-gather.3.cloned.1.call-update) | async-done | bytes 16777232 | tf_op jit(solution)/shard_map/all_gather | solution.py:13
  467.1 0.0 copy-done.1
  467.1 38.2 %convolution_convert_fusion = bf16[768,2048]{1,0:T(8,128)(2,1)} fusion(bf16[4096,2048]{1,0:T(8,128)(2,1)} %all-gather.5.cloned.1.call-done, bf16[2048,4096]{1,0:T(8,128)(2,1)} %all-gather.3.cloned.1.call-done, f32[2048]{0:T(1024)S(1)} %copy-done.1, f32[768]{0:T(1024)S(1)} %add_rsqrt_fusion, bf16[768,2048]{1,0:T(8,128)(2,1)S(1)} %copy-done), kind=kOutput, calls=%fused_computation.3 | convolution fusion | flops 25787105280 | bytes 39857152 | tf_op jit(solution)/shard_map/dot_general | solution.py:17
  505.2 0.0 reduce-scatter.2.cloned.1.call-update
  505.3 3.5 convert_element_type.18
  508.8 5.8 %reduce-scatter.2.cloned.1.call-done = bf16[768,1024]{1,0:T(8,128)(2,1)} async-done(((bf16[768,2048]{1,0:T(8,128)(2,1)}), bf16[768,1024]{1,0:T(8,128)(2,1)}) %reduce-scatter.2.cloned.1.call-update) | async-done | bytes 1572880 | tf_op jit(solution)/shard_map/reduce_scatter | solution.py:22
  514.5 4.1 add_convert_fusion
  (1 shorter events, 0.0 us)
Async XLA Ops:
  6.5 1.9 copy-start
  6.5 460.5 %copy-start.1 = (f32[2048]{0:T(1024)S(1)}, f32[2048]{0:T(1024)}, u32[]{:S(2)}) copy-start(f32[2048]{0:T(1024)} %param.5) | copy-start | bytes 24580
  6.5 232.9 %all-gather.5.cloned.1.call-start = ((), (), s32[]{:S(2)}) async-start(), calls=%async_computation.2 | async-start | bytes 18874368 | tf_op jit(solution)/shard_map/all_gather | solution.py:19
  7.3 459.8 %all-gather.3.cloned.1.call-start = ((), (), s32[]{:S(2)}) async-start(), calls=%async_computation.1 | async-start | bytes 18874368 | tf_op jit(solution)/shard_map/all_gather | solution.py:13
  8.0 506.5 %reduce-scatter.2.cloned.1.call-start = ((), (), s32[]{:S(2)}) async-start(), calls=%async_computation.3 | async-start | bytes 4718592 | tf_op jit(solution)/shard_map/reduce_scatter | solution.py:22
Sparse Core Ops, SparseCore 0:
  9.4 230.0 all-gather.4
  241.6 225.4 all-gather.2
  505.4 9.1 reduce-scatter.1
where the time goes:
time: 525 us
  waiting for transfers between devices  465 us (89%)
  matrix products  38.2 us (7%)
  between operations  13.1 us (2%)
  other arithmetic  8.27 us (2%)
    all_gather x1, waiting for transfers between devices, local(): lax.all_gather(down_weight, 'fs', axis=1, tiled=True)  230 us
    all_gather x1, waiting for transfers between devices, local(): lax.all_gather(up_weight, 'fs', axis=0, tiled=True)  228 us
    dot_general x1, matrix products, local(): jnp.dot(hidden, lax.all_gather(down_weight, 'fs', axis=1, tiled=True), pr...  38.2 us
  transfers between devices with their start and end apart: 3, of which 3 were waited for; matrix products, arithmetic and copies ran while one was open for 1% of the time, Pallas kernels for 0%

commit v1 on v0

v1 whole, which is shorter than its diff:
```python
import jax
import jax.numpy as jnp
from jax import lax
from jax.sharding import PartitionSpec as P


def local(tokens, norm_gain, up_weight, down_weight):
    n_rep = lax.axis_size("rep")
    rep = lax.axis_index("rep")
    ff = up_weight.shape[1] // n_rep
    up = lax.all_gather(
        lax.dynamic_slice_in_dim(up_weight, rep * ff, ff, 1), "fs", axis=0, tiled=True)
    down = lax.all_gather(
        lax.dynamic_slice_in_dim(down_weight, rep * ff, ff, 0), "fs", axis=1, tiled=True)
    xf = tokens.astype(jnp.float32)
    inv_rms = lax.rsqrt(jnp.mean(xf * xf, axis=-1, keepdims=True) + 1e-06)
    normed = (xf * inv_rms * norm_gain).astype(jnp.bfloat16)
    normed = lax.all_gather(normed, "rep", axis=0, tiled=True)
    pre = jnp.dot(normed, up, preferred_element_type=jnp.float32)
    hidden = jnp.square(jax.nn.relu(pre)).astype(jnp.bfloat16)
    terms = jnp.dot(hidden, down, preferred_element_type=jnp.float32).astype(jnp.bfloat16)
    summed = lax.psum_scatter(terms, "tp", scatter_dimension=1, tiled=True)
    summed = lax.psum_scatter(summed, "rep", scatter_dimension=0, tiled=True).astype(jnp.float32)
    width = summed.shape[1]
    own_cols = lax.dynamic_slice_in_dim(xf, lax.axis_index("tp") * width, width, 1)
    return (own_cols + summed).astype(jnp.bfloat16)


def solution(mesh):
    placed = (P(("rep", "fs"), None), P(), P("fs", "tp"), P("tp", "fs"))
    return jax.shard_map(
        local, mesh=mesh, in_specs=placed, out_specs=P(("rep", "fs"), "tp"), check_vma=False
    )
```

time: 525 us -> 453 us (0.86)
  waiting for transfers between devices: 465 us -> 385 us
  other arithmetic: 8.27 us -> 16.6 us
    all_gather x2 -> x3, waiting for transfers between devices: 458 us -> 332 us  [the longest x1 127 us: local(): lax.all_gather(lax.dynamic_slice_in_dim(up_weight, rep * ff, ff, 1), 'fs'...]
    reduce_scatter x1 -> x2, waiting for transfers between devices: 5.79 us -> 53.5 us  [the longest x1 41.4 us: local(): lax.psum_scatter(summed, 'rep', scatter_dimension=0, tiled=True)]
  transfers between devices with their start and end apart: 3 -> 5, of which waited for: 3 -> 5; matrix products, arithmetic and copies ran while one was open for 1% -> 2% of each run, Pallas kernels for 0% -> 0%
where the time goes in v1:
time: 453 us
  waiting for transfers between devices  385 us (85%)
  matrix products  34.7 us (8%)
  other arithmetic  16.6 us (4%)
  between operations  13.2 us (3%)
    all_gather x1, waiting for transfers between devices, local(): lax.all_gather(lax.dynamic_slice_in_dim(up_weight, rep * ff, ff, 1), 'fs'...  127 us
    all_gather x1, waiting for transfers between devices, local(): lax.all_gather(lax.dynamic_slice_in_dim(down_weight, rep * ff, ff, 0), 'f...  125 us
    all_gather x1, waiting for transfers between devices, local(): normed = lax.all_gather(normed, 'rep', axis=0, tiled=True)  79.7 us
    reduce_scatter x1, waiting for transfers between devices, local(): lax.psum_scatter(summed, 'rep', scatter_dimension=0, tiled=True)  41.4 us
    dot_general x1, matrix products, local(): jnp.dot(hidden, down, preferred_element_type=jnp.float32)  34.7 us
    reduce_scatter x1, waiting for transfers between devices, local(): summed = lax.psum_scatter(terms, 'tp', scatter_dimension=1, tiled=True)  12.1 us
  transfers between devices with their start and end apart: 5, of which 5 were waited for; matrix products, arithmetic and copies ran while one was open for 2% of the time, Pallas kernels for 0%

profile of v1, /device:TPU:0, one launch (start us, length us, event | category | flops | bytes accessed | tf_op | source)
XLA Modules:
  0.0 453.0 jit_solution(5884597010119765956)
XLA Ops:
  6.5 0.0 copy-start
  6.5 0.0 all-gather.4.cloned.1.call-start
  6.5 2.7 multiply_reduce_fusion
  9.3 4.4 multiply_convert_fusion.1
  13.7 0.0 all-gather.4.cloned.1.call-update
  13.7 0.0 all-gather.6.cloned.1.call-start
  13.7 0.0 copy-done
  13.7 1.1 constant_dynamic-slice_fusion.1
  14.8 0.0 all-gather.6.cloned.1.call-update
  14.8 0.0 all-gather.8.cloned.1.call-start
  14.9 2.3 constant_dynamic-slice_fusion
  17.2 0.0 all-gather.8.cloned.1.call-update
  17.2 0.0 reduce-scatter.3.cloned.1.call-start
  17.2 79.7 %all-gather.4.cloned.1.call-done = bf16[1536,2048]{1,0:T(8,128)(2,1)} async-done(((bf16[768,2048]{1,0:T(8,128)(2,1)}), bf16[1536,2048]{1,0:T(8,128)(2,1)}) %all-gather.4.cloned.1.call-update) | async-done | bytes 6291472 | tf_op jit(solution)/shard_map/all_gather | solution.py:18
  96.9 126.6 %all-gather.6.cloned.1.call-done = bf16[2048,2048]{1,0:T(8,128)(2,1)} async-done(((bf16[256,2048]{1,0:T(8,128)(2,1)}), bf16[2048,2048]{1,0:T(8,128)(2,1)}) %all-gather.6.cloned.1.call-update) | async-done | bytes 8388624 | tf_op jit(solution)/shard_map/all_gather | solution.py:11
  223.5 125.2 %all-gather.8.cloned.1.call-done = bf16[2048,2048]{1,0:T(8,128)(2,1)} async-done(((bf16[2048,256]{1,0:T(8,128)(2,1)}), bf16[2048,2048]{1,0:T(8,128)(2,1)}) %all-gather.8.cloned.1.call-update) | async-done | bytes 8388624 | tf_op jit(solution)/shard_map/all_gather | solution.py:13
  348.7 34.7 %fusion.1 = bf16[1536,2048]{1,0:T(8,128)(2,1)} fusion(bf16[2048,2048]{1,0:T(8,128)(2,1)} %all-gather.8.cloned.1.call-done, bf16[1536,2048]{1,0:T(8,128)(2,1)} %all-gather.4.cloned.1.call-done, bf16[2048,2048]{1,0:T(8,128)(2,1)} %all-gather.6.cloned.1.call-done), kind=kOutput, calls=%fused_computation.2 | convolution fusion | flops 25782386688 | bytes 29360128 | tf_op jit(solution)/shard_map/dot_general | solution.py:21
  383.4 0.0 reduce-scatter.3.cloned.1.call-update
  383.4 0.0 reduce-scatter.5.cloned.1.call-start
  383.5 12.1 %reduce-scatter.3.cloned.1.call-done = bf16[1536,1024]{1,0:T(8,128)(2,1)} async-done(((bf16[1536,2048]{1,0:T(8,128)(2,1)}), bf16[1536,1024]{1,0:T(8,128)(2,1)}) %reduce-scatter.3.cloned.1.call-update) | async-done | bytes 3145744 | tf_op jit(solution)/shard_map/reduce_scatter | solution.py:22
  395.6 0.0 reduce-scatter.5.cloned.1.call-update
  395.6 5.4 %convert_element_type.18 = f32[768,2048]{1,0:T(8,128)} convert(bf16[768,2048]{1,0:T(8,128)(2,1)} %param.4) | non-fusion elementwise | flops 1572864 | bytes 9437184 | tf_op jit(solution)/shard_map/convert_element_type | solution.py:15
  401.0 41.4 %reduce-scatter.5.cloned.1.call-done = bf16[768,1024]{1,0:T(8,128)(2,1)} async-done(((bf16[1536,1024]{1,0:T(8,128)(2,1)}), bf16[768,1024]{1,0:T(8,128)(2,1)}) %reduce-scatter.5.cloned.1.call-update) | async-done | bytes 1572880 | tf_op jit(solution)/shard_map/reduce_scatter | solution.py:23
  442.4 4.1 add_convert_fusion
  (1 shorter events, 0.0 us)
Async XLA Ops:
  6.5 7.2 %copy-start = (bf16[256,4096]{1,0:T(8,128)(2,1)S(1)}, bf16[256,4096]{1,0:T(8,128)(2,1)}, u32[]{:S(2)}) copy-start(bf16[256,4096]{1,0:T(8,128)(2,1)} %param.6) | copy-start | bytes 6291460
  6.5 90.4 %all-gather.4.cloned.1.call-start = ((), (), s32[]{:S(2)}) async-start(), calls=%async_computation.2 | async-start | bytes 9437184 | tf_op jit(solution)/shard_map/all_gather | solution.py:18
  13.7 209.9 %all-gather.6.cloned.1.call-start = ((), (), s32[]{:S(2)}) async-start(), calls=%async_computation.3 | async-start | bytes 9437184 | tf_op jit(solution)/shard_map/all_gather | solution.py:11
  14.8 333.9 %all-gather.8.cloned.1.call-start = ((), (), s32[]{:S(2)}) async-start(), calls=%async_computation.4 | async-start | bytes 9437184 | tf_op jit(solution)/shard_map/all_gather | solution.py:13
  17.2 378.4 %reduce-scatter.3.cloned.1.call-start = ((), (), s32[]{:S(2)}) async-start(), calls=%async_computation.5 | async-start | bytes 9437184 | tf_op jit(solution)/shard_map/reduce_scatter | solution.py:22
  383.4 59.0 %reduce-scatter.5.cloned.1.call-start = ((), (), s32[]{:S(2)}) async-start(), calls=%async_computation.6 | async-start | bytes 4718592 | tf_op jit(solution)/shard_map/reduce_scatter | solution.py:23
Sparse Core Ops, SparseCore 0:
  13.8 83.0 all-gather.3
  99.0 124.4 all-gather.5
  225.6 123.1 all-gather.7
  383.5 12.0 reduce-scatter.2
  397.7 44.6 reduce-scatter.4

commit v2 on v1

v2 whole, which is shorter than its diff:
```python
import functools

import jax
import jax.numpy as jnp
from jax import lax
from jax.experimental import pallas as pl
from jax.experimental.pallas import tpu as pltpu
from jax.sharding import PartitionSpec as P

MESH = pl.DeviceIdType.MESH
F32 = jnp.float32
BF16 = jnp.bfloat16


def kernel(nz, normed, up, down, out, T, acc, hid, U, Dn, Pr, Ar, Br, fin, loc, tok_s, tok_r,
           wy_s, wy_r, z_s, z_r, d_s, d_r, a_s, a_r, b_s, b_r, f_s, f_r):
    x, f, c = lax.axis_index("rep"), lax.axis_index("fs"), lax.axis_index("tp")
    z, y = f // 2, f % 2
    half, blk = T.shape[3], T.shape[4]
    wide = U.shape[2]
    row = blk // 2
    own = x * 2 + y
    ax, ay = (x + 1 - c) % 2, (y + c) % 2
    bx, by = (x + c) % 2, (y + 1 - c) % 2
    q_a, q_b, q_ab = ax * 2 + ay, bx * 2 + by, (1 - x) * 2 + 1 - y
    to_a = {"rep": ax, "fs": z * 2 + ay}
    to_b = {"rep": bx, "fs": z * 2 + by}
    to_y = {"fs": z * 2 + 1 - y}
    to_x = {"rep": 1 - x}
    to_c = {"tp": 1 - c}
    above = {"fs": jnp.minimum(z + 1, nz - 1) * 2 + y}
    below = {"fs": jnp.maximum(z - 1, 0) * 2 + y}
    has_above, has_below = z < nz - 1, z > 0

    def remote(src, dst, s, r, dev):
        return pltpu.make_async_remote_copy(
            src_ref=src, dst_ref=dst, send_sem=s, recv_sem=r, device_id=dev, device_id_type=MESH)

    def order(s):
        m = jnp.minimum(z, nz - 1 - z)
        near = z - (s + 1) // 2 if s % 2 else z + s // 2
        far = jnp.where(z < nz - 1 - z, s, nz - 1 - s)
        return jnp.where(s <= 2 * m, near, far)

    barrier = pltpu.get_barrier_semaphore()
    for dev in (to_x, to_y, to_c):
        pl.semaphore_signal(barrier, inc=1, device_id=dev, device_id_type=MESH)

    @pl.when(has_above)
    def _():
        pl.semaphore_signal(barrier, inc=1, device_id=above, device_id_type=MESH)

    @pl.when(has_below)
    def _():
        pl.semaphore_signal(barrier, inc=1, device_id=below, device_id_type=MESH)

    locals_ = []
    for k in range(nz):
        for h in range(2):
            locals_.append(pltpu.make_async_copy(
                normed.at[pl.ds(h * half, half), pl.ds(k * blk, blk)],
                T.at[k, own, h], loc.at[k * 2 + h]))
    slot = (lambda zz, p: U.at[zz, pl.ds(pl.multiple_of(p * row, row), row)],
            lambda zz, p: Dn.at[zz, :, pl.ds(pl.multiple_of(p * row, row), row)])
    part = (lambda q: up.at[:, pl.ds(pl.multiple_of(q * wide, wide), wide)],
            lambda q: down.at[pl.ds(pl.multiple_of(q * wide, wide), wide)])
    for w in range(2):
        locals_.append(pltpu.make_async_copy(part[w](own), slot[w](z, y), loc.at[2 * nz + w]))
    for copy in locals_:
        copy.start()
    pl.semaphore_wait(barrier, 3 + jnp.where(has_above, 1, 0) + jnp.where(has_below, 1, 0))

    swap = [remote(part[w](x * 2 + 1 - y), slot[w](z, y), wy_s.at[w], wy_r.at[w], to_y)
            for w in range(2)]

    def hop(w, upward, zz, p):
        return remote(slot[w](zz, p), slot[w](zz, p), z_s.at[w, 0 if upward else 1, zz, p],
                      z_r.at[w, zz, p], above if upward else below)

    def send(w, zz, p, act="start"):
        @pl.when(jnp.logical_and(has_above, zz <= z))
        def _():
            hop(w, True, zz, p).start() if act == "start" else hop(w, True, zz, p).wait_send()

        @pl.when(jnp.logical_and(has_below, zz >= z))
        def _():
            hop(w, False, zz, p).start() if act == "start" else hop(w, False, zz, p).wait_send()

    def pieces(w):
        return (y, 1 - y) if w == 0 else (0, 1)

    def arrive(w, s):
        zz = order(s)
        for p in pieces(w):
            hop(w, True, zz, p).wait_recv()
            send(w, zz, p)

    def piece(q):
        return T.at[:, q, c]

    tok = [remote(piece(own), piece(own), tok_s.at[0], tok_r.at[0], to_a),
           remote(piece(own), piece(own), tok_s.at[1], tok_r.at[1], to_b),
           remote(piece(q_a), piece(q_a), tok_s.at[2], tok_r.at[2], to_b)]
    tok += [remote(piece(q), piece(q), tok_s.at[3 + i], tok_r.at[3 + i], to_c)
            for i, q in enumerate((q_a, q_b, q_ab))]

    swap[0].start()
    locals_[2 * nz].wait()
    send(0, z, y)
    for copy in locals_[:2 * nz]:
        copy.wait()
    tok[0].start()
    tok[1].start()
    swap[1].start()
    swap[0].wait_recv()
    send(0, z, 1 - y)
    arrive(0, 1)
    tok[0].wait_recv()
    tok[2].start()
    tok[3].start()
    tok[1].wait_recv()
    tok[4].start()
    for s in range(2, nz - 1):
        arrive(0, s)
    locals_[2 * nz + 1].wait()
    swap[1].wait_recv()
    send(1, z, 0)
    send(1, z, 1)
    tok[2].wait_recv()
    tok[5].start()
    for i in range(3):
        tok[3 + i].wait_recv()
    for copy in tok:
        copy.wait_send()
    if nz > 2:
        arrive(1, 1)

    def up_block(s):
        zz = order(s)

        @pl.loop(0, 8)
        def _(i):
            q, h = i // 2, i % 2
            term = jnp.dot(T[zz, q, h], U[zz], preferred_element_type=F32)
            if s > 0:
                term += acc[q, h]
            if s < nz - 1:
                acc[q, h] = term
            else:
                hid[q, h] = jnp.square(jnp.maximum(term, 0.0)).astype(BF16)

    for s in range(nz):
        if s == nz - 1:
            arrive(0, s)
        up_block(s)

    def stage_a(s):
        zz = order(s)
        for h in (1 - c, c):
            @pl.loop(0, 4)
            def _(q):
                T[zz, q, h] = jnp.dot(
                    hid[q, h], Dn[zz], preferred_element_type=F32).astype(BF16)
            if h is not c:
                d2d(s).start()

    def d2d(s):
        zz = order(s)
        return remote(T.at[zz, :, 1 - c], Pr.at[zz], d_s.at[zz], d_r.at[zz], to_c)

    def to_first(s, i):
        zz = order(s)
        return remote(T.at[zz, (q_a, q_ab)[i], c], Ar.at[zz, i], a_s.at[zz, i], a_r.at[zz, i],
                      to_a)

    def to_second(s):
        zz = order(s)
        return remote(T.at[zz, q_b, c], Br.at[zz], b_s.at[zz], b_r.at[zz], to_b)

    def finish(s):
        zz = order(s)
        return remote(T.at[zz, own, c], fin.at[zz % (nz // 2), c], f_s.at[zz], f_r.at[zz], to_c)

    def stage_b(s):
        zz = order(s)
        d2d(s).wait_recv()
        for i, q in ((1, q_ab), (0, q_a), (2, q_b), (3, own)):
            T[zz, q, c] = (T[zz, q, c].astype(F32) + Pr[zz, q].astype(F32)).astype(BF16)
            if i < 2:
                to_first(s, i).start()

    def stage_c(s):
        zz = order(s)
        to_first(s, 1).wait_recv()
        T[zz, q_b, c] = (T[zz, q_b, c].astype(F32) + Ar[zz, 1].astype(F32)).astype(BF16)
        to_second(s).start()

    def stage_d(s):
        zz = order(s)
        to_first(s, 0).wait_recv()
        to_second(s).wait_recv()
        T[zz, own, c] = (T[zz, own, c].astype(F32) + Ar[zz, 0].astype(F32)
                         + Br[zz].astype(F32)).astype(BF16)

        @pl.when(zz // (nz // 2) == c)
        def _():
            fin[zz % (nz // 2), c] = T[zz, own, c]

        @pl.when(zz // (nz // 2) != c)
        def _():
            finish(s).start()

    for s in range(nz):
        if s > 1 or (s == 1 and nz == 2):
            arrive(1, s)
        stage_a(s)
        if s:
            stage_c(s - 1)
        stage_b(s)
        if s:
            stage_d(s - 1)
    stage_c(nz - 1)
    stage_d(nz - 1)

    for s in range(nz):
        zz = order(s)

        @pl.when(zz // (nz // 2) == c)
        def _():
            finish(s).wait_recv()

        @pl.when(zz // (nz // 2) != c)
        def _():
            finish(s).wait_send()
    outs = [pltpu.make_async_copy(
        fin.at[k, h], out.at[pl.ds(h * half, half), pl.ds(k * blk, blk)], loc.at[k * 2 + h])
        for k in range(nz // 2) for h in range(2)]
    for copy in outs:
        copy.start()
    for w in range(2):
        swap[w].wait_send()
        for s in range(nz):
            for p in pieces(w):
                send(w, order(s), p, "wait")
    for s in range(nz):
        d2d(s).wait_send()
        to_first(s, 0).wait_send()
        to_first(s, 1).wait_send()
        to_second(s).wait_send()
    for copy in outs:
        copy.wait()


def fused(nz, normed, up, down):
    rows, d = normed.shape
    wide = up.shape[1] // 4
    half, blk = rows // 2, d // nz
    sem = pltpu.SemaphoreType.DMA
    return pl.pallas_call(
        functools.partial(kernel, nz),
        out_shape=jax.ShapeDtypeStruct((rows, d // 2), BF16),
        in_specs=[pl.BlockSpec(memory_space=pl.ANY)] * 3,
        out_specs=pl.BlockSpec(memory_space=pl.ANY),
        scratch_shapes=[
            pltpu.VMEM((nz, 4, 2, half, blk), BF16),
            pltpu.VMEM((4, 2, half, wide), F32),
            pltpu.VMEM((4, 2, half, wide), BF16),
            pltpu.VMEM((nz, blk, wide), BF16),
            pltpu.VMEM((nz, wide, blk), BF16),
            pltpu.VMEM((nz, 4, half, blk), BF16),
            pltpu.VMEM((nz, 2, half, blk), BF16),
            pltpu.VMEM((nz, half, blk), BF16),
            pltpu.VMEM((nz // 2, 2, half, blk), BF16),
            sem((2 * nz + 2,)), sem((6,)), sem((6,)), sem((2,)), sem((2,)),
            sem((2, 2, nz, 2)), sem((2, nz, 2)), sem((nz,)), sem((nz,)),
            sem((nz, 2)), sem((nz, 2)), sem((nz,)), sem((nz,)), sem((nz,)), sem((nz,)),
        ],
        compiler_params=pltpu.CompilerParams(
            collective_id=0, has_side_effects=True, vmem_limit_bytes=60 * 2**20),
    )(normed, up, down)


def spread(normed, up_weight, down_weight):
    n_rep = lax.axis_size("rep")
    rep = lax.axis_index("rep")
    ff = up_weight.shape[1] // n_rep
    up = lax.all_gather(
        lax.dynamic_slice_in_dim(up_weight, rep * ff, ff, 1), "fs", axis=0, tiled=True)
    down = lax.all_gather(
        lax.dynamic_slice_in_dim(down_weight, rep * ff, ff, 0), "fs", axis=1, tiled=True)
    normed = lax.all_gather(normed, "rep", axis=0, tiled=True)
    pre = jnp.dot(normed, up, preferred_element_type=F32)
    hidden = jnp.square(jax.nn.relu(pre)).astype(BF16)
    terms = jnp.dot(hidden, down, preferred_element_type=F32).astype(BF16)
    summed = lax.psum_scatter(terms, "tp", scatter_dimension=1, tiled=True)
    return lax.psum_scatter(summed, "rep", scatter_dimension=0, tiled=True)


def local(tokens, norm_gain, up_weight, down_weight):
    xf = tokens.astype(F32)
    inv_rms = lax.rsqrt(jnp.mean(xf * xf, axis=-1, keepdims=True) + 1e-06)
    normed = (xf * inv_rms * norm_gain).astype(BF16)
    n_rep, n_fs, n_tp = (lax.axis_size(a) for a in ("rep", "fs", "tp"))
    if n_rep == 2 and n_tp == 2 and n_fs % 4 == 0:
        summed = fused(n_fs // 2, normed, up_weight, down_weight)
    else:
        summed = spread(normed, up_weight, down_weight)
    summed = summed.astype(F32)
    width = summed.shape[1]
    own_cols = lax.dynamic_slice_in_dim(xf, lax.axis_index("tp") * width, width, 1)
    return (own_cols + summed).astype(BF16)


def solution(mesh):
    placed = (P(("rep", "fs"), None), P(), P("fs", "tp"), P("tp", "fs"))
    return jax.shard_map(
        local, mesh=mesh, in_specs=placed, out_specs=P(("rep", "fs"), "tp"), check_vma=False
    )
```

time: 453 us -> 220 us (0.49)
  waiting for transfers between devices: 385 us -> 0 us
  Pallas kernels: 0 us -> 212 us
  matrix products: 34.7 us -> 0 us
  between operations: 13.2 us -> 0.03 us
  other arithmetic: 16.6 us -> 7.71 us
    all_gather x3 -> x0, waiting for transfers between devices: 332 us -> none  [the longest x1 127 us: local(): lax.all_gather(lax.dynamic_slice_in_dim(up_weight, rep * ff, ff, 1), 'fs'...]
    pallas_call x0 -> x1, Pallas kernels: none -> 212 us  [fused(): pl.pallas_call(functools.partial(kernel, nz), out_shape=jax.ShapeDtypeStr...]
    reduce_scatter x2 -> x0, waiting for transfers between devices: 53.5 us -> none  [the longest x1 41.4 us: local(): lax.psum_scatter(summed, 'rep', scatter_dimension=0, tiled=True)]
    dot_general x1 -> x0, matrix products: 34.7 us -> none  [local(): jnp.dot(hidden, down, preferred_element_type=jnp.float32)]
    convert_element_type x3, other arithmetic: 13.9 us -> 4.99 us  [the longest x1 2.44 us: local(): normed = (xf * inv_rms * norm_gain).astype(BF16)]
  transfers between devices with their start and end apart: 5 -> 0, of which waited for: 5 -> 0; matrix products, arithmetic and copies ran while one was open for 2% -> 0% of each run, Pallas kernels for 0% -> 0%
where the time goes in v2:
time: 220 us
  Pallas kernels  212 us (96%)
  other arithmetic  7.71 us (4%)
    pallas_call x1, Pallas kernels, fused(): pl.pallas_call(functools.partial(kernel, nz), out_shape=jax.ShapeDtypeStr...  212 us

profile of v2, /device:TPU:0, one launch (start us, length us, event | category | flops | bytes accessed | tf_op | source)
XLA Modules:
  0.0 220.3 jit_solution(9046321932780155502)
XLA Ops:
  0.0 0.0 copy-start
  0.0 0.0 copy-start.2
  0.0 2.7 %multiply_reduce_fusion = f32[768]{0:T(1024)S(1)} fusion(bf16[768,2048]{1,0:T(8,128)(2,1)} %param.4), kind=kLoop, calls=%fused_computation.1 | loop fusion | flops 4717824 | bytes 3148800 | tf_op jit(solution)/shard_map/reduce_sum | solution.py:301
  2.7 0.1 copy-done
  2.8 0.0 copy-done.2
  2.8 2.4 %multiply_convert_fusion.normed = bf16[768,2048]{1,0:T(8,128)(2,1)} fusion(f32[2048]{0:T(1024)S(1)} %copy-done.2, f32[768]{0:T(1024)S(1)} %add_rsqrt_fusion, bf16[768,2048]{1,0:T(8,128)(2,1)S(1)} %copy-done), kind=kLoop, calls=%fused_computation | loop fusion | flops 6291456 | bytes 6302720 | tf_op jit(solution)/shard_map/convert_element_type | solution.py:302
  5.3 211.9 %shard_map.46 = bf16[768,1024]{1,0:T(8,128)(2,1)} custom-call(bf16[768,2048]{1,0:T(8,128)(2,1)} %multiply_convert_fusion.normed, bf16[256,4096]{1,0:T(8,128)(2,1)} %up.1, bf16[4096,256]{1,0:T(8,128)(2,1)} %down.1), custom_call_target="tpu_custom_call" | custom-call | tf_op jit(solution)/shard_map/pallas_call | solution.py:259
  217.2 0.0 copy-start.1
  217.2 0.8 convert_element_type.12
  218.0 0.6 copy-done.1
  218.6 1.7 add_convert_fusion
  (1 shorter events, 0.0 us)
Async XLA Ops:
  0.0 2.8 %copy-start = (bf16[768,2048]{1,0:T(8,128)(2,1)S(1)}, bf16[768,2048]{1,0:T(8,128)(2,1)}, u32[]{:S(2)}) copy-start(bf16[768,2048]{1,0:T(8,128)(2,1)} %param.4) | copy-start | bytes 9437188
  0.0 2.8 %copy-start.2 = (f32[2048]{0:T(1024)S(1)}, f32[2048]{0:T(1024)}, u32[]{:S(2)}) copy-start(f32[2048]{0:T(1024)} %param.5) | copy-start | bytes 24580
  217.2 1.4 copy-start.1

commit v3 on v2

--- a/solution.py
+++ b/solution.py
@@ -86,14 +86,24 @@
         def _():
             hop(w, False, zz, p).start() if act == "start" else hop(w, False, zz, p).wait_send()
 
+    inner = jnp.logical_and(has_above, has_below)
+
     def pieces(w):
         return (y, 1 - y) if w == 0 else (0, 1)
 
-    def arrive(w, s):
-        zz = order(s)
-        for p in pieces(w):
-            hop(w, True, zz, p).wait_recv()
-            send(w, zz, p)
+    def relay(w, s):
+        if s < nz:
+            zz = order(s)
+            for p in pieces(w):
+                @pl.when(inner)
+                def _():
+                    hop(w, True, zz, p).wait_recv()
+                send(w, zz, p)
+
+    def arrived(w, s, p):
+        @pl.when(jnp.logical_not(inner))
+        def _():
+            hop(w, True, order(s), p).wait_recv()
 
     def piece(q):
         return T.at[:, q, c]
@@ -104,43 +114,11 @@
     tok += [remote(piece(q), piece(q), tok_s.at[3 + i], tok_r.at[3 + i], to_c)
             for i, q in enumerate((q_a, q_b, q_ab))]
 
-    swap[0].start()
-    locals_[2 * nz].wait()
-    send(0, z, y)
-    for copy in locals_[:2 * nz]:
-        copy.wait()
-    tok[0].start()
-    tok[1].start()
-    swap[1].start()
-    swap[0].wait_recv()
-    send(0, z, 1 - y)
-    arrive(0, 1)
-    tok[0].wait_recv()
-    tok[2].start()
-    tok[3].start()
-    tok[1].wait_recv()
-    tok[4].start()
-    for s in range(2, nz - 1):
-        arrive(0, s)
-    locals_[2 * nz + 1].wait()
-    swap[1].wait_recv()
-    send(1, z, 0)
-    send(1, z, 1)
-    tok[2].wait_recv()
-    tok[5].start()
-    for i in range(3):
-        tok[3 + i].wait_recv()
-    for copy in tok:
-        copy.wait_send()
-    if nz > 2:
-        arrive(1, 1)
-
-    def up_block(s):
-        zz = order(s)
-
-        @pl.loop(0, 8)
-        def _(i):
-            q, h = i // 2, i % 2
+    def up_block(q, s):
+        zz = order(s)
+
+        @pl.loop(0, 2)
+        def _(h):
             term = jnp.dot(T[zz, q, h], U[zz], preferred_element_type=F32)
             if s > 0:
                 term += acc[q, h]
@@ -149,89 +127,147 @@
             else:
                 hid[q, h] = jnp.square(jnp.maximum(term, 0.0)).astype(BF16)
 
+    swap[0].start()
+    swap[1].start()
+    locals_[2 * nz].wait()
+    send(0, z, y)
+    for copy in locals_[:2 * nz]:
+        copy.wait()
+    tok[0].start()
+    tok[1].start()
+    swap[0].wait_recv()
+    send(0, z, 1 - y)
+    relay(0, 1)
+    relay(0, 2)
+    tok[0].wait_recv()
+    tok[2].start()
+    tok[3].start()
+    locals_[2 * nz + 1].wait()
+    swap[1].wait_recv()
+    for s in range(3, nz):
+        relay(0, s)
+    send(1, z, 0)
+    send(1, z, 1)
+    up_block(own, 0)
+    for p in pieces(0):
+        arrived(0, 1, p)
+    up_block(own, 1)
+    tok[1].wait_recv()
+    tok[4].start()
+    for q, i in ((q_a, 4), (q_b, 3)):
+        tok[i].wait_recv()
+        up_block(q, 0)
+        up_block(q, 1)
+    relay(1, 1)
+    for s in range(2, nz):
+        for p in pieces(0):
+            arrived(0, s, p)
+        if s < nz - 1:
+            for q in (own, q_a, q_b):
+                up_block(q, s)
+    relay(1, 2)
+    tok[2].wait_recv()
+    tok[5].start()
+    if nz > 2:
+        for q in (own, q_a, q_b):
+            up_block(q, nz - 1)
+    tok[5].wait_recv()
     for s in range(nz):
-        if s == nz - 1:
-            arrive(0, s)
-        up_block(s)
-
-    def stage_a(s):
+        up_block(q_ab, s)
+    for s in range(3, nz):
+        relay(1, s)
+    for copy in tok:
+        copy.wait_send()
+
+    def cols(p):
+        return pl.ds(p * row, row)
+
+    def d2d(s, p):
+        zz = order(s)
+        return remote(T.at[zz, :, 1 - c, :, cols(p)], Pr.at[zz, :, :, cols(p)],
+                      d_s.at[zz, p], d_r.at[zz, p], to_c)
+
+    def to_first(s, p, i):
+        zz = order(s)
+        return remote(T.at[zz, (q_a, q_ab)[i], c, :, cols(p)], Ar.at[zz, i, :, cols(p)],
+                      a_s.at[zz, p, i], a_r.at[zz, p, i], to_a)
+
+    def to_second(s, p):
+        zz = order(s)
+        return remote(T.at[zz, q_b, c, :, cols(p)], Br.at[zz, :, cols(p)],
+                      b_s.at[zz, p], b_r.at[zz, p], to_b)
+
+    def finish(s, p):
+        zz = order(s)
+        return remote(T.at[zz, own, c, :, cols(p)], fin.at[zz % (nz // 2), c, :, cols(p)],
+                      f_s.at[zz, p], f_r.at[zz, p], to_c)
+
+    def stage_a(s, p):
         zz = order(s)
         for h in (1 - c, c):
             @pl.loop(0, 4)
             def _(q):
-                T[zz, q, h] = jnp.dot(
-                    hid[q, h], Dn[zz], preferred_element_type=F32).astype(BF16)
+                T[zz, q, h, :, cols(p)] = jnp.dot(
+                    hid[q, h], Dn[zz, :, cols(p)], preferred_element_type=F32).astype(BF16)
             if h is not c:
-                d2d(s).start()
-
-    def d2d(s):
-        zz = order(s)
-        return remote(T.at[zz, :, 1 - c], Pr.at[zz], d_s.at[zz], d_r.at[zz], to_c)
-
-    def to_first(s, i):
-        zz = order(s)
-        return remote(T.at[zz, (q_a, q_ab)[i], c], Ar.at[zz, i], a_s.at[zz, i], a_r.at[zz, i],
-                      to_a)
-
-    def to_second(s):
-        zz = order(s)
-        return remote(T.at[zz, q_b, c], Br.at[zz], b_s.at[zz], b_r.at[zz], to_b)
-
-    def finish(s):
-        zz = order(s)
-        return remote(T.at[zz, own, c], fin.at[zz % (nz // 2), c], f_s.at[zz], f_r.at[zz], to_c)
-
-    def stage_b(s):
-        zz = order(s)
-        d2d(s).wait_recv()
+                d2d(s, p).start()
+
+    def stage_b(s, p):
+        zz, k = order(s), cols(p)
+        d2d(s, p).wait_recv()
         for i, q in ((1, q_ab), (0, q_a), (2, q_b), (3, own)):
-            T[zz, q, c] = (T[zz, q, c].astype(F32) + Pr[zz, q].astype(F32)).astype(BF16)
+            T[zz, q, c, :, k] = (
+                T[zz, q, c, :, k].astype(F32) + Pr[zz, q, :, k].astype(F32)).astype(BF16)
             if i < 2:
-                to_first(s, i).start()
-
-    def stage_c(s):
-        zz = order(s)
-        to_first(s, 1).wait_recv()
-        T[zz, q_b, c] = (T[zz, q_b, c].astype(F32) + Ar[zz, 1].astype(F32)).astype(BF16)
-        to_second(s).start()
-
-    def stage_d(s):
-        zz = order(s)
-        to_first(s, 0).wait_recv()
-        to_second(s).wait_recv()
-        T[zz, own, c] = (T[zz, own, c].astype(F32) + Ar[zz, 0].astype(F32)
-                         + Br[zz].astype(F32)).astype(BF16)
+                to_first(s, p, i).start()
+
+    def stage_c(s, p):
+        zz, k = order(s), cols(p)
+        to_first(s, p, 1).wait_recv()
+        T[zz, q_b, c, :, k] = (
+            T[zz, q_b, c, :, k].astype(F32) + Ar[zz, 1, :, k].astype(F32)).astype(BF16)
+        to_second(s, p).start()
+
+    def stage_d(s, p):
+        zz, k = order(s), cols(p)
+        to_first(s, p, 0).wait_recv()
+        to_second(s, p).wait_recv()
+        T[zz, own, c, :, k] = (
+            T[zz, own, c, :, k].astype(F32) + Ar[zz, 0, :, k].astype(F32)
+            + Br[zz, :, k].astype(F32)).astype(BF16)
 
         @pl.when(zz // (nz // 2) == c)
         def _():
-            fin[zz % (nz // 2), c] = T[zz, own, c]
+            fin[zz % (nz // 2), c, :, k] = T[zz, own, c, :, k]
 
         @pl.when(zz // (nz // 2) != c)
         def _():
-            finish(s).start()
-
-    for s in range(nz):
-        if s > 1 or (s == 1 and nz == 2):
-            arrive(1, s)
-        stage_a(s)
+            finish(s, p).start()
+
+    steps = [(s, p) for s in range(nz) for p in range(2)]
+    for n, (s, p) in enumerate(steps):
         if s:
-            stage_c(s - 1)
-        stage_b(s)
-        if s:
-            stage_d(s - 1)
-    stage_c(nz - 1)
-    stage_d(nz - 1)
-
-    for s in range(nz):
+            arrived(1, s, p)
+        stage_a(s, p)
+        if n:
+            stage_c(*steps[n - 1])
+        stage_b(s, p)
+        if n > 1:
+            stage_d(*steps[n - 2])
+    stage_d(*steps[-2])
+    stage_c(*steps[-1])
+    stage_d(*steps[-1])
+
+    for s, p in steps:
         zz = order(s)
 
         @pl.when(zz // (nz // 2) == c)
         def _():
-            finish(s).wait_recv()
+            finish(s, p).wait_recv()
 
         @pl.when(zz // (nz // 2) != c)
         def _():
-            finish(s).wait_send()
+            finish(s, p).wait_send()
     outs = [pltpu.make_async_copy(
         fin.at[k, h], out.at[pl.ds(h * half, half), pl.ds(k * blk, blk)], loc.at[k * 2 + h])
         for k in range(nz // 2) for h in range(2)]
@@ -242,11 +278,11 @@
         for s in range(nz):
             for p in pieces(w):
                 send(w, order(s), p, "wait")
-    for s in range(nz):
-        d2d(s).wait_send()
-        to_first(s, 0).wait_send()
-        to_first(s, 1).wait_send()
-        to_second(s).wait_send()
+    for s, p in steps:
+        d2d(s, p).wait_send()
+        to_first(s, p, 0).wait_send()
+        to_first(s, p, 1).wait_send()
+        to_second(s, p).wait_send()
     for copy in outs:
         copy.wait()
 
@@ -272,8 +308,9 @@
             pltpu.VMEM((nz, half, blk), BF16),
             pltpu.VMEM((nz // 2, 2, half, blk), BF16),
             sem((2 * nz + 2,)), sem((6,)), sem((6,)), sem((2,)), sem((2,)),
-            sem((2, 2, nz, 2)), sem((2, nz, 2)), sem((nz,)), sem((nz,)),
-            sem((nz, 2)), sem((nz, 2)), sem((nz,)), sem((nz,)), sem((nz,)), sem((nz,)),
+            sem((2, 2, nz, 2)), sem((2, nz, 2)), sem((nz, 2)), sem((nz, 2)),
+            sem((nz, 2, 2)), sem((nz, 2, 2)), sem((nz, 2)), sem((nz, 2)), sem((nz, 2)),
+            sem((nz, 2)),
         ],
         compiler_params=pltpu.CompilerParams(
             collective_id=0, has_side_effects=True, vmem_limit_bytes=60 * 2**20),

time: 220 us -> 170 us (0.77)
  Pallas kernels: 212 us -> 161 us
    pallas_call x1, Pallas kernels: 212 us -> 161 us  [fused(): pl.pallas_call(functools.partial(kernel, nz), out_shape=jax.ShapeDtypeStr...]
where the time goes in v3:
time: 170 us
  Pallas kernels  161 us (95%)
  other arithmetic  7.71 us (5%)
    pallas_call x1, Pallas kernels, fused(): pl.pallas_call(functools.partial(kernel, nz), out_shape=jax.ShapeDtypeStr...  161 us

profile of v3, /device:TPU:0, one launch (start us, length us, event | category | flops | bytes accessed | tf_op | source)
XLA Modules:
  0.0 169.9 jit_solution(8624677188120161613)
XLA Ops:
  0.0 0.0 copy-start
  0.0 0.0 copy-start.2
  0.0 2.7 %multiply_reduce_fusion = f32[768]{0:T(1024)S(1)} fusion(bf16[768,2048]{1,0:T(8,128)(2,1)} %param.4), kind=kLoop, calls=%fused_computation.1 | loop fusion | flops 4717824 | bytes 3148800 | tf_op jit(solution)/shard_map/reduce_sum | solution.py:338
  2.7 0.1 copy-done
  2.8 0.0 copy-done.2
  2.8 2.4 %multiply_convert_fusion.normed = bf16[768,2048]{1,0:T(8,128)(2,1)} fusion(f32[2048]{0:T(1024)S(1)} %copy-done.2, f32[768]{0:T(1024)S(1)} %add_rsqrt_fusion, bf16[768,2048]{1,0:T(8,128)(2,1)S(1)} %copy-done), kind=kLoop, calls=%fused_computation | loop fusion | flops 6291456 | bytes 6302720 | tf_op jit(solution)/shard_map/convert_element_type | solution.py:339
  5.3 161.5 %shard_map.46 = bf16[768,1024]{1,0:T(8,128)(2,1)} custom-call(bf16[768,2048]{1,0:T(8,128)(2,1)} %multiply_convert_fusion.normed, bf16[256,4096]{1,0:T(8,128)(2,1)} %up.1, bf16[4096,256]{1,0:T(8,128)(2,1)} %down.1), custom_call_target="tpu_custom_call" | custom-call | tf_op jit(solution)/shard_map/pallas_call | solution.py:295
  166.8 0.0 copy-start.1
  166.8 0.8 convert_element_type.12
  167.6 0.6 copy-done.1
  168.2 1.7 %add_convert_fusion = bf16[768,1024]{1,0:T(8,128)(2,1)} fusion(bf16[768,1024]{1,0:T(8,128)(2,1)S(1)} %copy-done.1, f32[768,2048]{1,0:T(8,128)S(1)} %convert_element_type.12, s32[]{:T(128)S(6)} %select_n.3), kind=kLoop, calls=%fused_computation.2 | loop fusion | flops 2359296 | bytes 6291460 | tf_op jit(solution)/shard_map/convert_element_type | solution.py:348
  (1 shorter events, 0.0 us)
Async XLA Ops:
  0.0 2.8 %copy-start = (bf16[768,2048]{1,0:T(8,128)(2,1)S(1)}, bf16[768,2048]{1,0:T(8,128)(2,1)}, u32[]{:S(2)}) copy-start(bf16[768,2048]{1,0:T(8,128)(2,1)} %param.4) | copy-start | bytes 9437188
  0.0 2.8 %copy-start.2 = (f32[2048]{0:T(1024)S(1)}, f32[2048]{0:T(1024)}, u32[]{:S(2)}) copy-start(f32[2048]{0:T(1024)} %param.5) | copy-start | bytes 24580
  166.8 1.4 copy-start.1
